TPU v7x, 512 devices: a whole 4x8x8 slice. The times are simulated.
512 devices in a mesh: fs: 64 (over z, y), tp: 8 (over x, core).
Axes of the slice: x: 4, y: 8, z: 8, core: 2. Of those that a mesh axis runs over, the one named last changes fastest.
Arguments:
- prompt: bfloat16 [20480, 2048], P('fs', 'tp'), may hold values from -6 to 6
- norm_gain: float32 [2048], P('fs'), may hold values from 0.1 to 1.9
- gate_master: float32 [2048, 3072], P('fs', 'tp'), may hold values from -0.125 to 0.125
- up_master: float32 [2048, 3072], P('fs', 'tp'), may hold values from -0.125 to 0.125
- down_master: float32 [2048, 3072], P('fs', 'tp'), may hold values from -0.109375 to 0.109375
Outputs:
- gate_new: bfloat16 [3072, 2048], P('tp')
- up_new: bfloat16 [3072, 2048], P('tp')
- down_new: bfloat16 [3072, 2048], P('tp')
- mixed: bfloat16 [2048, 20480], P('tp', 'fs')
All inputs are finite; a program needn't handle non-finite values.
Results may differ from a plain program's by a relative error of at most 0.0082.
Values may be sent and summed in bfloat16 or wider, within the bound.
No kernel may reach another device: no remote copies, remote signals or barrier semaphores. Data moves between devices by JAX's collectives and lax.ppermute only.
A program may use at most 64 MiB of HBM per device.

v0:
```python
import jax
import jax.numpy as jnp
from jax import lax
from jax.sharding import PartitionSpec as P


def laid_out(parts, dim):
    parts = jnp.moveaxis(parts, 0, dim)
    shape = parts.shape
    return parts.reshape(*shape[:dim], shape[dim] * shape[dim + 1], *shape[dim + 2 :])


def sent_to_all(array, axis):
    copies = jnp.broadcast_to(array, (lax.axis_size(axis), *array.shape))
    return lax.all_to_all(copies, axis, split_axis=0, concat_axis=0, tiled=True)


def gathered_copies(array, axis, dim):
    return laid_out(sent_to_all(array, axis), dim)


def gather_turned(arrays, axis, dims):
    turned = [jnp.moveaxis(a, dim, 0) for a, dim in zip(arrays, dims)]
    widths = [t[0].size for t in turned]
    both = jnp.concatenate([t.reshape(-1, w) for t, w in zip(turned, widths)], axis=1)
    filled = lax.all_gather(both, axis, axis=0, tiled=True)
    parts = jnp.split(filled, [sum(widths[:k]) for k in range(1, len(widths))], axis=1)
    return tuple(
        (
            jnp.moveaxis(b.reshape(-1, *t.shape[1:]), 0, dim)
            for b, t, dim in zip(parts, turned, dims)
        )
    )


def cut_along(array, dim, size):
    before, after = (array.shape[:dim], array.shape[dim + 1 :])
    return jnp.moveaxis(array.reshape(*before, size, -1, *after), dim, 0)


def sent_and_summed(array, axis, dim):
    parts = cut_along(array, dim, lax.axis_size(axis))
    arrived = lax.all_to_all(parts, axis, split_axis=0, concat_axis=0, tiled=True)
    return arrived.astype(jnp.float32).sum(axis=0)


def on_device(prompt, norm_gain, gate_master, up_master, down_master):
    gain_col = norm_gain[:, None]
    gate_low = (gate_master * gain_col).astype(jnp.bfloat16).T
    up_low = (up_master * gain_col).astype(jnp.bfloat16).T
    down_low = down_master.astype(jnp.bfloat16).T
    whole = gathered_copies(prompt, "tp", 1)
    values = whole.astype(jnp.float32)
    normed = (values * lax.rsqrt(jnp.mean(values * values, axis=1, keepdims=True) + 1e-06)).astype(
        jnp.bfloat16
    )
    contract = (((1,), (1,)), ((), ()))
    gate_new, up_new, down_new = gather_turned((gate_low, up_low, down_low), "fs", (1, 1, 1))
    gate = lax.dot_general(normed, gate_new, contract, preferred_element_type=jnp.float32)
    up = lax.dot_general(normed, up_new, contract, preferred_element_type=jnp.float32)
    hidden = (jax.nn.silu(gate) * up).astype(jnp.bfloat16)
    mixed = sent_and_summed(
        lax.dot_general(
            down_new, hidden, (((0,), (1,)), ((), ())), preferred_element_type=jnp.float32
        ).astype(jnp.bfloat16),
        "tp",
        0,
    )
    return (gate_new, up_new, down_new, mixed.astype(jnp.bfloat16))


def solution(mesh):
    placed = (P("fs", "tp"), P("fs"), P("fs", "tp"), P("fs", "tp"), P("fs", "tp"))
    return jax.shard_map(
        on_device,
        mesh=mesh,
        in_specs=placed,
        out_specs=(P("tp", None), P("tp", None), P("tp", None), P("tp", "fs")),
        check_vma=False,
    )
```

profile of v0, /device:TPU:1, one launch (start us, length us, event | category | flops | bytes accessed | tf_op | source)
XLA Modules:
  0.0 145.5 jit_solution(8326352939495786494)
XLA Ops:
  7.2 0.0 all-gather.2.cloned.1.call-start
  7.2 0.8 convert_element_type.35
  8.0 0.9 multiply_convert_fusion.2
  8.9 0.6 pad_maximum_fusion
  9.6 0.0 all-gather.2.cloned.1.call-update
  9.6 1.0 broadcast_in_dim.2
  10.6 27.0 %all_to_all.10 = bf16[8,320,256]{2,1,0:T(8,128)(2,1)S(1)} all-to-all(bf16[8,320,256]{2,1,0:T(8,128)(2,1)S(1)} %broadcast_in_dim.2), channel_id=1, replica_groups=mesh['fs'=64,'tp'=8] {'tp'}, dimensions={0} | all-to-all | bytes 2621440 | tf_op jit(solution)/shard_map/all_to_all | solution.py:15
  37.6 0.2 convert_bitcast_fusion
  37.8 0.3 copy.21
  38.2 0.4 fusion
  38.6 61.7 %all-gather.2.cloned.1.call-done = bf16[2048,1152]{1,0:T(8,128)(2,1)} async-done(((bf16[32,1152]{1,0:T(8,128)(2,1)}), bf16[2048,1152]{1,0:T(8,128)(2,1)}) %all-gather.2.cloned.1.call-update) | async-done | bytes 4718608 | tf_op jit(solution)/shard_map/all_gather | solution.py:26
  100.3 2.3 %fusion.4 = f32[320,384]{1,0:T(8,128)S(1)} fusion(bf16[2048,1152]{1,0:T(8,128)(2,1)} %all-gather.2.cloned.1.call-done, f32[320,2048]{1,0:T(8,128)S(1)} %bitcast.14, f32[320]{0:T(512)S(1)} %add_rsqrt_fusion), kind=kOutput, calls=%fused_computation.10 | convolution fusion | flops 504627200 | bytes 4687104 | tf_op jit(solution)/shard_map/dot_general | solution.py:59
  102.6 4.6 %convolution_convert_fusion = bf16[2048,320]{0,1:T(8,128)(2,1)} fusion(bf16[2048,1152]{1,0:T(8,128)(2,1)} %all-gather.2.cloned.1.call-done, f32[320,384]{1,0:T(8,128)S(1)} %fusion.4, f32[320,2048]{1,0:T(8,128)S(1)} %bitcast.15, f32[320]{0:T(512)S(1)} %add_rsqrt_fusion), kind=kOutput, calls=%fused_computation.2 | convolution fusion | flops 1009336320 | bytes 7570688 | tf_op jit(solution)/shard_map/dot_general | solution.py:63
  107.2 2.5 %copy.23 = bf16[40,8,8,256]{3,2,0,1:T(8,128)(2,1)} copy(bf16[40,8,8,256]{3,2,1,0:T(8,128)(2,1)} %bitcast.16) | data formatting | bytes 2621440 | tf_op jit(solution)/shard_map/reshape | solution.py:38
  109.7 8.9 %all-to-all-start.1 = ((bf16[8,256,320]{1,2,0:T(8,128)(2,1)}), bf16[8,256,320]{1,2,0:T(8,128)(2,1)}, u32[]{:S(2)}, u32[]{:S(2)}) async-start(bf16[8,256,320]{1,2,0:T(8,128)(2,1)} %bitcast.13), calls=%async_computation.1 | async-start | bytes 2621440 | tf_op jit(solution)/shard_map/all_to_all | solution.py:43
  118.6 4.0 %slice_bitcast_fusion = (bf16[384,2048]{0,1:T(8,128)(2,1)}, bf16[384,2048]{0,1:T(8,128)(2,1)S(1)}, bf16[384,2048]{0,1:T(8,128)(2,1)S(1)}) fusion(bf16[2048,1152]{1,0:T(8,128)(2,1)} %all-gather.2.cloned.1.call-done), kind=kLoop, calls=%fused_computation.6 | loop fusion | bytes 9437184 | tf_op jit(solution)/shard_map/transpose | solution.py:30
  122.6 2.6 %copy.19 = bf16[384,2048]{1,0:T(8,128)(2,1)} copy(bf16[384,2048]{0,1:T(8,128)(2,1)} %get-tuple-element.8) | data formatting | bytes 3145728
  125.2 1.6 %copy.18 = bf16[384,2048]{1,0:T(8,128)(2,1)} copy(bf16[384,2048]{0,1:T(8,128)(2,1)S(1)} %get-tuple-element.9) | data formatting | bytes 3145728
  126.8 1.6 %copy.17 = bf16[384,2048]{1,0:T(8,128)(2,1)} copy(bf16[384,2048]{0,1:T(8,128)(2,1)S(1)} %get-tuple-element.10) | data formatting | bytes 3145728
  128.4 8.1 %all-to-all-done.1 = bf16[8,256,320]{1,2,0:T(8,128)(2,1)} async-done(((bf16[8,256,320]{1,2,0:T(8,128)(2,1)}), bf16[8,256,320]{1,2,0:T(8,128)(2,1)}, u32[]{:S(2)}, u32[]{:S(2)}) %all-to-all-start.1) | async-done | bytes 1310752 | tf_op jit(solution)/shard_map/all_to_all | solution.py:43
  136.5 2.2 %reduce_sum.22 = bf16[256,320]{0,1:T(8,128)(2,1)} reduce(bf16[8,256,320]{1,2,0:T(8,128)(2,1)} %all-to-all-done.1, bf16[]{:T(256)} %constant.11.clone.1), dimensions={0}, to_apply=%region_1.2 | reduce | flops 573440 | bytes 1474562 | tf_op jit(solution)/shard_map/reduce_sum | solution.py:44
  (1 shorter events, 0.0 us)
Async XLA Ops:
  7.2 93.1 %all-gather.2.cloned.1.call-start = ((), (), s32[]{:S(2)}) async-start(), calls=%async_computation.2 | async-start | bytes 4792320 | tf_op jit(solution)/shard_map/all_gather | solution.py:26
  109.7 26.8 %all-to-all-start.1 = ((bf16[8,256,320]{1,2,0:T(8,128)(2,1)}), bf16[8,256,320]{1,2,0:T(8,128)(2,1)}, u32[]{:S(2)}, u32[]{:S(2)}) async-start(bf16[8,256,320]{1,2,0:T(8,128)(2,1)} %bitcast.13), calls=%async_computation.1 | async-start | bytes 2621440 | tf_op jit(solution)/shard_map/all_to_all | solution.py:43
Sparse Core Ops, SparseCore 0:
  11.6 88.6 all-gather.1
where the time goes:
time: 146 us
  waiting for transfers between devices  69.8 us (48%)
  blocking collectives  27 us (18%)
  between operations  14.1 us (10%)
  local copies, waits for them, and re-layouts  13.7 us (9%)
  starting transfers between devices  8.97 us (6%)
  matrix products  6.86 us (5%)
  other arithmetic  5.16 us (4%)
    all_gather x1, waiting for transfers between devices, gather_turned(): filled = lax.all_gather(both, axis, axis=0, tiled=True)  61.7 us
    all_to_all x1, blocking collectives, sent_to_all(): return lax.all_to_all(copies, axis, split_axis=0, concat_axis=0, tiled=True)  27 us
    all_to_all x1, starting transfers between devices, sent_and_summed(): lax.all_to_all(parts, axis, split_axis=0, concat_axis=0, tiled=True)  8.93 us
    all_to_all x1, waiting for transfers between devices, sent_and_summed(): lax.all_to_all(parts, axis, split_axis=0, concat_axis=0, tiled=True)  8.07 us
    unnamed x3, local copies, waits for them, and re-layouts  5.81 us
    dot_general x1, matrix products, on_device(): lax.dot_general(down_new, hidden, (((0,), (1,)), ((), ())), preferred_ele...  4.58 us
    transpose x1, local copies, waits for them, and re-layouts, gather_turned(): jnp.moveaxis(b.reshape(-1, *t.shape[1:]), 0, dim)  4 us
  transfers between devices with their start and end apart: 2, of which 2 were waited for; matrix products, arithmetic and copies ran while one was open for 8% of the time, Pallas kernels for 0%

commit v1 on v0

--- a/solution.py
+++ b/solution.py
@@ -23,7 +23,9 @@
     turned = [jnp.moveaxis(a, dim, 0) for a, dim in zip(arrays, dims)]
     widths = [t[0].size for t in turned]
     both = jnp.concatenate([t.reshape(-1, w) for t, w in zip(turned, widths)], axis=1)
-    filled = lax.all_gather(both, axis, axis=0, tiled=True)
+    filled = jnp.concatenate(
+        lax.all_to_all(jnp.stack([both] * lax.axis_size(axis)), axis, 0, 0), axis=0
+    )
     parts = jnp.split(filled, [sum(widths[:k]) for k in range(1, len(widths))], axis=1)
     return tuple(
         (

time: 146 us -> 228 us (1.56)
  the two profiles are of different devices: /device:TPU:1 before, /device:TPU:40 now
where the time goes in v1:
time: 228 us; the launch traced here: 227 us
  waiting for transfers between devices  170 us (75%)
  starting transfers between devices  28.1 us (12%)
  local copies, waits for them, and re-layouts  18.3 us (8%)
  matrix products  6.86 us (3%)
  other arithmetic  2.89 us (1%)
    all_to_all x1, waiting for transfers between devices, gather_turned(): lax.all_to_all(jnp.stack([both] * lax.axis_size(axis)), axis, 0, 0)  143 us
    all_to_all x1, waiting for transfers between devices, sent_to_all(): return lax.all_to_all(copies, axis, split_axis=0, concat_axis=0, tiled=True)  18.6 us
    all_to_all x1, starting transfers between devices, gather_turned(): lax.all_to_all(jnp.stack([both] * lax.axis_size(axis)), axis, 0, 0)  16.3 us
    all_to_all x1, waiting for transfers between devices, sent_and_summed(): lax.all_to_all(parts, axis, split_axis=0, concat_axis=0, tiled=True)  9.04 us
    all_to_all x1, starting transfers between devices, sent_and_summed(): lax.all_to_all(parts, axis, split_axis=0, concat_axis=0, tiled=True)  7.34 us
    unnamed x15, local copies, waits for them, and re-layouts  6.78 us
    dot_general x1, matrix products, on_device(): lax.dot_general(down_new, hidden, (((0,), (1,)), ((), ())), preferred_ele...  4.58 us
  transfers between devices with their start and end apart: 3, of which 3 were waited for; matrix products, arithmetic and copies ran while one was open for 5% of the time, Pallas kernels for 0%

profile of v1, /device:TPU:40, one launch (start us, length us, event | category | flops | bytes accessed | tf_op | source)
XLA Modules:
  0.0 227.1 jit_solution(6413101152671446926)
XLA Ops:
  0.6 2.1 broadcast_in_dim.2
  2.7 0.0 copy-start.2
  2.7 0.0 copy-start.3
  2.7 0.0 copy-start.4
  2.7 0.0 copy-start.5
  2.7 4.4 %all-to-all-start.1 = ((bf16[8,320,256]{2,1,0:T(8,128)(2,1)}), bf16[8,320,256]{2,1,0:T(8,128)(2,1)S(1)}, u32[]{:S(2)}, u32[]{:S(2)}) async-start(bf16[8,320,256]{2,1,0:T(8,128)(2,1)} %broadcast_in_dim.2), calls=%async_computation.1 | async-start | bytes 2621440 | tf_op jit(solution)/shard_map/all_to_all | solution.py:15
  7.1 0.0 copy-done.2
  7.2 0.0 copy-done.3
  7.2 0.0 copy-done.4
  7.2 0.0 copy-done.5
  7.2 0.1 multiply_convert_fusion.2
  7.3 18.6 %all-to-all-done.1 = bf16[8,320,256]{2,1,0:T(8,128)(2,1)S(1)} async-done(((bf16[8,320,256]{2,1,0:T(8,128)(2,1)}), bf16[8,320,256]{2,1,0:T(8,128)(2,1)S(1)}, u32[]{:S(2)}, u32[]{:S(2)}) %all-to-all-start.1) | async-done | bytes 1310752 | tf_op jit(solution)/shard_map/all_to_all | solution.py:15
  25.9 0.0 copy-start
  25.9 2.6 %stack.2 = bf16[64,32,1152]{2,1,0:T(8,128)(2,1)} broadcast(bf16[32,1152]{1,0:T(8,128)(2,1)S(1)} %pad_maximum_fusion), dimensions={1,2} | broadcast | bytes 4792320 | tf_op jit(solution)/shard_map/stack | solution.py:27
  28.5 16.3 %all-to-all-start = ((bf16[64,32,1152]{2,1,0:T(8,128)(2,1)}), bf16[64,32,1152]{2,1,0:T(8,128)(2,1)}, u32[]{:S(2)}, u32[]{:S(2)}) async-start(bf16[64,32,1152]{2,1,0:T(8,128)(2,1)} %stack.2), calls=%async_computation | async-start | bytes 9437184 | tf_op jit(solution)/shard_map/all_to_all | solution.py:27
  44.8 0.0 copy-done
  44.8 0.2 convert_bitcast_fusion
  45.0 0.0 copy-start.1
  45.1 0.3 copy.19
  45.4 0.9 copy-done.1
  46.4 0.4 fusion
  46.7 142.7 %all-to-all-done = bf16[64,32,1152]{2,1,0:T(8,128)(2,1)} async-done(((bf16[64,32,1152]{2,1,0:T(8,128)(2,1)}), bf16[64,32,1152]{2,1,0:T(8,128)(2,1)}, u32[]{:S(2)}, u32[]{:S(2)}) %all-to-all-start) | async-done | bytes 4718624 | tf_op jit(solution)/shard_map/all_to_all | solution.py:27
  189.4 2.3 %fusion.4 = f32[320,384]{1,0:T(8,128)S(1)} fusion(bf16[2048,1152]{1,0:T(8,128)(2,1)} %bitcast, f32[320,2048]{1,0:T(8,128)S(1)} %bitcast.15, f32[320]{0:T(512)S(1)} %add_rsqrt_fusion), kind=kOutput, calls=%fused_computation.10 | convolution fusion | flops 504627200 | bytes 4687104 | tf_op jit(solution)/shard_map/dot_general | solution.py:61
  191.7 4.6 %convolution_convert_fusion = bf16[2048,320]{0,1:T(8,128)(2,1)} fusion(bf16[2048,1152]{1,0:T(8,128)(2,1)} %bitcast, f32[320,384]{1,0:T(8,128)S(1)} %fusion.4, f32[320,2048]{1,0:T(8,128)S(1)} %bitcast.16, f32[320]{0:T(512)S(1)} %add_rsqrt_fusion), kind=kOutput, calls=%fused_computation.2 | convolution fusion | flops 1009336320 | bytes 7570688 | tf_op jit(solution)/shard_map/dot_general | solution.py:65
  196.3 2.5 %copy.21 = bf16[40,8,8,256]{3,2,0,1:T(8,128)(2,1)} copy(bf16[40,8,8,256]{3,2,1,0:T(8,128)(2,1)} %bitcast.17) | data formatting | bytes 2621440 | tf_op jit(solution)/shard_map/reshape | solution.py:40
  198.8 7.3 %all-to-all-start.2 = ((bf16[8,256,320]{1,2,0:T(8,128)(2,1)}), bf16[8,256,320]{1,2,0:T(8,128)(2,1)}, u32[]{:S(2)}, u32[]{:S(2)}) async-start(bf16[8,256,320]{1,2,0:T(8,128)(2,1)} %bitcast.14), calls=%async_computation.2 | async-start | bytes 2621440 | tf_op jit(solution)/shard_map/all_to_all | solution.py:45
  206.1 4.0 %slice_bitcast_fusion = (bf16[384,2048]{0,1:T(8,128)(2,1)S(1)}, bf16[384,2048]{0,1:T(8,128)(2,1)S(1)}, bf16[384,2048]{0,1:T(8,128)(2,1)}) fusion(bf16[2048,1152]{1,0:T(8,128)(2,1)} %bitcast), kind=kLoop, calls=%fused_computation.6 | loop fusion | bytes 9437184 | tf_op jit(solution)/shard_map/transpose | solution.py:32
  210.1 2.6 %copy.15 = bf16[384,2048]{1,0:T(8,128)(2,1)} copy(bf16[384,2048]{0,1:T(8,128)(2,1)} %get-tuple-element.14) | data formatting | bytes 3145728
  212.7 1.6 copy.16
  214.3 1.6 copy.17
  215.9 9.0 %all-to-all-done.2 = bf16[8,256,320]{1,2,0:T(8,128)(2,1)} async-done(((bf16[8,256,320]{1,2,0:T(8,128)(2,1)}), bf16[8,256,320]{1,2,0:T(8,128)(2,1)}, u32[]{:S(2)}, u32[]{:S(2)}) %all-to-all-start.2) | async-done | bytes 1310752 | tf_op jit(solution)/shard_map/all_to_all | solution.py:45
  224.9 2.2 reduce_sum.22
  (3 shorter events, 0.0 us)
Async XLA Ops:
  2.7 4.5 %copy-start.2 = (f32[32,384]{1,0:T(8,128)S(1)}, f32[32,384]{1,0:T(8,128)}, u32[]{:S(2)}) copy-start(f32[32,384]{1,0:T(8,128)} %param.9) | copy-start | bytes 147460
  2.7 4.5 %copy-start.3 = (f32[32,384]{1,0:T(8,128)S(1)}, f32[32,384]{1,0:T(8,128)}, u32[]{:S(2)}) copy-start(f32[32,384]{1,0:T(8,128)} %param.7) | copy-start | bytes 147460
  2.7 4.5 %copy-start.4 = (f32[32,384]{1,0:T(8,128)S(1)}, f32[32,384]{1,0:T(8,128)}, u32[]{:S(2)}) copy-start(f32[32,384]{1,0:T(8,128)} %param.8) | copy-start | bytes 147460
  2.7 4.5 %copy-start.5 = (f32[32]{0:T(128)S(1)}, f32[32]{0:T(128)}, u32[]{:S(2)}) copy-start(f32[32]{0:T(128)} %param.6) | copy-start | bytes 388
  2.7 23.2 %all-to-all-start.1 = ((bf16[8,320,256]{2,1,0:T(8,128)(2,1)}), bf16[8,320,256]{2,1,0:T(8,128)(2,1)S(1)}, u32[]{:S(2)}, u32[]{:S(2)}) async-start(bf16[8,320,256]{2,1,0:T(8,128)(2,1)} %broadcast_in_dim.2), calls=%async_computation.1 | async-start | bytes 2621440 | tf_op jit(solution)/shard_map/all_to_all | solution.py:15
  25.9 18.9 %copy-start = (bf16[8,320,256]{2,1,0:T(8,128)(2,1)}, bf16[8,320,256]{2,1,0:T(8,128)(2,1)S(1)}, u32[]{:S(2)}) copy-start(bf16[8,320,256]{2,1,0:T(8,128)(2,1)S(1)} %all-to-all-done.1) | copy-start | bytes 3932164
  28.5 160.9 %all-to-all-start = ((bf16[64,32,1152]{2,1,0:T(8,128)(2,1)}), bf16[64,32,1152]{2,1,0:T(8,128)(2,1)}, u32[]{:S(2)}, u32[]{:S(2)}) async-start(bf16[64,32,1152]{2,1,0:T(8,128)(2,1)} %stack.2), calls=%async_computation | async-start | bytes 9437184 | tf_op jit(solution)/shard_map/all_to_all | solution.py:27
  45.0 1.3 copy-start.1
  198.8 26.2 %all-to-all-start.2 = ((bf16[8,256,320]{1,2,0:T(8,128)(2,1)}), bf16[8,256,320]{1,2,0:T(8,128)(2,1)}, u32[]{:S(2)}, u32[]{:S(2)}) async-start(bf16[8,256,320]{1,2,0:T(8,128)(2,1)} %bitcast.14), calls=%async_computation.2 | async-start | bytes 2621440 | tf_op jit(solution)/shard_map/all_to_all | solution.py:45
